TPU v7x, 32 devices: a whole 2x2x4 slice. The times are simulated.
32 devices in a mesh: fs: 4 (over z), tp: 4 (over y, x), rep: 2 (over core).
Axes of the slice: x: 2, y: 2, z: 4, core: 2. Of those that a mesh axis runs over, the one named last changes fastest.
Arguments:
- gate_weight: float32 [2048, 5632], P('fs', 'tp'), may hold values from -6 to 6
- gate_momentum: float32 [2048, 5632], P('fs', 'tp'), may hold values from -60 to 60
- gate_grads: float32 [2, 2048, 5632], P('rep', 'fs', 'tp'), may hold values from -3500 to 3500
- gate_rows: float32 [2048], P('fs'), may hold values from 0.3 to 3
- gate_columns: float32 [5632], P('tp'), may hold values from 0.3 to 3
- up_weight: float32 [2048, 5632], P('fs', 'tp'), may hold values from -6 to 6
- up_momentum: float32 [2048, 5632], P('fs', 'tp'), may hold values from -60 to 60
- up_grads: float32 [2, 2048, 5632], P('rep', 'fs', 'tp'), may hold values from -3500 to 3500
- up_rows: float32 [2048], P('fs'), may hold values from 0.3 to 3
- up_columns: float32 [5632], P('tp'), may hold values from 0.3 to 3
- down_weight: float32 [5632, 2048], P('fs', 'tp'), may hold values from -6 to 6
- down_momentum: float32 [5632, 2048], P('fs', 'tp'), may hold values from -60 to 60
- down_grads: float32 [2, 5632, 2048], P('rep', 'fs', 'tp'), may hold values from -3500 to 3500
- down_rows: float32 [5632], P('fs'), may hold values from 0.3 to 3
- down_columns: float32 [2048], P('tp'), may hold values from 0.3 to 3
- mixer_weight: float32 [2048, 2048], P('fs', 'tp'), may hold values from -6 to 6
- mixer_momentum: float32 [2048, 2048], P('fs', 'tp'), may hold values from -60 to 60
- mixer_grads: float32 [2, 2048, 2048], P('rep', 'fs', 'tp'), may hold values from -3500 to 3500
- mixer_rows: float32 [2048], P('fs'), may hold values from 0.3 to 3
- mixer_columns: float32 [2048], P('tp'), may hold values from 0.3 to 3
Outputs:
- gate_weight_next: float32 [2048, 5632], P('fs', 'tp')
- gate_momentum_next: float32 [2048, 5632], P('fs', 'tp')
- gate_rows_next: float32 [2048], P('fs')
- gate_columns_next: float32 [5632], P('tp')
- up_weight_next: float32 [2048, 5632], P('fs', 'tp')
- up_momentum_next: float32 [2048, 5632], P('fs', 'tp')
- up_rows_next: float32 [2048], P('fs')
- up_columns_next: float32 [5632], P('tp')
- down_weight_next: float32 [5632, 2048], P('fs', 'tp')
- down_momentum_next: float32 [5632, 2048], P('fs', 'tp')
- down_rows_next: float32 [5632], P('fs')
- down_columns_next: float32 [2048], P('tp')
- mixer_weight_next: float32 [2048, 2048], P('fs', 'tp')
- mixer_momentum_next: float32 [2048, 2048], P('fs', 'tp')
- mixer_rows_next: float32 [2048], P('fs')
- mixer_columns_next: float32 [2048], P('tp')
All inputs are finite; a program needn't handle non-finite values.
Results may differ from a plain program's by a relative error of at most 0.00002.
Values sent between devices are 32-bit elements; how exact they have to be, the bound alone decides.
A program may use at most 128 MiB of HBM per device.

v0:
```python
import jax
import jax.numpy as jnp
from jax import lax
from jax.sharding import PartitionSpec as P

momentum_decay = 0.9
moment_decay = 0.95
clip_level = 0.25
step_rate = 0.1


def body(
    gate_weight,
    gate_momentum,
    gate_grads,
    gate_rows,
    gate_columns,
    up_weight,
    up_momentum,
    up_grads,
    up_rows,
    up_columns,
    down_weight,
    down_momentum,
    down_grads,
    down_rows,
    down_columns,
    mixer_weight,
    mixer_momentum,
    mixer_grads,
    mixer_rows,
    mixer_columns,
):
    weights = (gate_weight, up_weight, down_weight, mixer_weight)
    momenta = (gate_momentum, up_momentum, down_momentum, mixer_momentum)
    partials = (gate_grads, up_grads, down_grads, mixer_grads)
    rows = (gate_rows, up_rows, down_rows, mixer_rows)
    columns = (gate_columns, up_columns, down_columns, mixer_columns)
    summed = lax.psum((partials[0], partials[1], partials[2], partials[3]), "rep")
    column_count = [item.shape[1] * lax.axis_size("tp") for item in weights]
    grads = [item[0] for item in summed]
    row_count = [item.shape[0] * lax.axis_size("fs") for item in weights]
    momenta_next = [momentum_decay * m + (1.0 - momentum_decay) * g for m, g in zip(momenta, grads)]
    squares = [g * g for g in grads]
    row_local = tuple((jnp.sum(item, axis=1) for item in squares))
    row_total = lax.psum(row_local, "tp")
    rows_next = [
        moment_decay * r + (1.0 - moment_decay) * t / n
        for r, t, n in zip(rows, row_total, column_count)
    ]
    column_local = tuple((jnp.sum(item, axis=0) for item in squares))
    row_mass = tuple((jnp.sum(item) for item in rows_next))
    shares = tuple((jnp.sum(m * m / r[:, None], axis=0) for m, r in zip(momenta_next, rows_next)))
    outcome = lax.psum(column_local + row_mass + shares, "fs")
    columns_next = [
        moment_decay * c + (1.0 - moment_decay) * outcome[k] / row_count[k]
        for k, c in enumerate(columns)
    ]
    row_means = [outcome[4 + k] / row_count[k] for k in range(4)]
    updates = [
        m * lax.rsqrt(r[:, None] * c[None, :] / q)
        for m, r, c, q in zip(momenta_next, rows_next, columns_next, row_means)
    ]
    pieces = tuple((row_means[k] * jnp.sum(outcome[8 + k] / columns_next[k]) for k in range(4)))
    totals = lax.psum(pieces, "tp")
    weights_next = []
    for k in range(4):
        spread = jnp.sqrt(totals[k] / (row_count[k] * column_count[k]))
        factor = jnp.maximum(1.0, spread / clip_level)
        weights_next.append(weights[k] - step_rate * updates[k] / factor)
    return (
        weights_next[0],
        momenta_next[0],
        rows_next[0],
        columns_next[0],
        weights_next[1],
        momenta_next[1],
        rows_next[1],
        columns_next[1],
        weights_next[2],
        momenta_next[2],
        rows_next[2],
        columns_next[2],
        weights_next[3],
        momenta_next[3],
        rows_next[3],
        columns_next[3],
    )


def solution(mesh):
    return jax.shard_map(
        body,
        mesh=mesh,
        in_specs=(
            P("fs", "tp"),
            P("fs", "tp"),
            P("rep", "fs", "tp"),
            P("fs"),
            P("tp"),
            P("fs", "tp"),
            P("fs", "tp"),
            P("rep", "fs", "tp"),
            P("fs"),
            P("tp"),
            P("fs", "tp"),
            P("fs", "tp"),
            P("rep", "fs", "tp"),
            P("fs"),
            P("tp"),
            P("fs", "tp"),
            P("fs", "tp"),
            P("rep", "fs", "tp"),
            P("fs"),
            P("tp"),
        ),
        out_specs=(
            P("fs", "tp"),
            P("fs", "tp"),
            P("fs"),
            P("tp"),
            P("fs", "tp"),
            P("fs", "tp"),
            P("fs"),
            P("tp"),
            P("fs", "tp"),
            P("fs", "tp"),
            P("fs"),
            P("tp"),
            P("fs", "tp"),
            P("fs", "tp"),
            P("fs"),
            P("tp"),
        ),
        check_vma=False,
    )
```

profile of v0, /device:TPU:0, one launch (start us, length us, event | category | flops | bytes accessed | tf_op | source)
XLA Modules:
  0.0 147.0 jit_solution(8685572275804125372)
XLA Ops:
  7.2 0.0 all-reduce.6.cloned.1.call-start
  7.2 0.7 all-reduce.6.cloned.1.call-update
  7.9 46.9 %all-reduce.6.cloned.1.call-done = (f32[1,512,1408]{2,1,0:T(8,128)}, f32[1,512,1408]{2,1,0:T(8,128)}, f32[1,1408,512]{2,1,0:T(8,128)}, f32[1,512,512]{2,1,0:T(8,128)}) async-done(((f32[1,512,1408]{2,1,0:T(8,128)}, f32[1,512,1408]{2,1,0:T(8,128)}, f32[1,1408,512]{2,1,0:T(8,128)}, f32[1,512,512]{2,1,0:T(8,128)}), (f32[1,512,1408]{2,1,0:T(8,128)}, f32[1,512,1408]{2,1,0:T(8,128)}, f32[1,1408,512]{2,1,0:T(8,128)}, ...) | async-done | bytes 9699344 | tf_op jit(solution)/shard_map/psum | solution.py:39
  54.8 1.6 %multiply_reduce_fusion.6 = (f32[512]{0:T(512)S(1)}, f32[512]{0:T(512)S(1)}) fusion(f32[1,512,512]{2,1,0:T(8,128)} %get-tuple-element.47), kind=kLoop, calls=%fused_computation.22 | loop fusion | flops 785408 | bytes 1052672 | tf_op jit(solution)/shard_map/reduce_sum | solution.py:51
  56.4 2.4 %multiply_reduce_fusion.4 = (f32[1408]{0:T(1024)S(1)}, f32[512]{0:T(512)S(1)}) fusion(f32[1,512,1408]{2,1,0:T(8,128)} %get-tuple-element.44), kind=kLoop, calls=%fused_computation.16 | loop fusion | flops 2160768 | bytes 2891264 | tf_op jit(solution)/shard_map/reduce_sum | solution.py:51
  58.8 0.4 multiply_reduce_fusion.2
  59.2 0.0 copy-done.3
  59.2 0.4 multiply_reduce_fusion
  59.5 16.5 %all-reduce.1 = (f32[512]{0:T(512)S(1)}, f32[512]{0:T(512)S(1)}, f32[1408]{0:T(1024)S(1)}, f32[512]{0:T(512)S(1)}) all-reduce(f32[512]{0:T(512)S(1)} %get-tuple-element.21, f32[512]{0:T(512)S(1)} %get-tuple-element.19, f32[1408]{0:T(1024)S(1)} %get-tuple-element.17, ...), channel_id=1, replica_groups=mesh['fs'=4,'tp'=4,'rep'=2] {'tp'}, use_global_device_ids=true, to_apply=%region_2.0 | all-reduce | flops 2944 | bytes 23552 | tf_op jit(solution)/shard_map/psum | solution.py:46
  76.0 0.6 fusion.7
  76.6 0.6 fusion.4
  77.2 1.2 fusion.3
  78.5 2.6 %fusion.1 = (f32[1408]{0:T(1024)S(1)}, f32[512,1408]{1,0:T(8,128)S(1)}) fusion(f32[512]{0:T(512)S(1)} %get-tuple-element.73, f32[1,512,1408]{2,1,0:T(8,128)} %get-tuple-element.45, f32[512,1408]{1,0:T(8,128)S(1)} %copy-done.8), kind=kLoop, calls=%fused_computation.10 | loop fusion | flops 4323968 | bytes 8658432 | tf_op jit(solution)/shard_map/reduce_sum | solution.py:53
  81.1 0.1 copy-done.5
  81.1 0.9 copy-done.9
  82.0 2.2 %fusion = (f32[1408]{0:T(1024)S(1)}, f32[512,1408]{1,0:T(8,128)}) fusion(f32[512]{0:T(512)S(1)} %get-tuple-element.71, f32[1,512,1408]{2,1,0:T(8,128)S(1)} %copy-done.5, f32[512,1408]{1,0:T(8,128)S(1)} %copy-done.9), kind=kLoop, calls=%fused_computation.9 | loop fusion | flops 4323968 | bytes 8658432 | tf_op jit(solution)/shard_map/reduce_sum | solution.py:53
  84.2 0.6 fusion.5
  84.8 1.0 copy-done.10
  85.8 2.2 %fusion.2 = (f32[512]{0:T(512)S(1)}, f32[1408,512]{1,0:T(8,128)}) fusion(f32[1408]{0:T(1024)S(1)} %get-tuple-element.63, f32[1,1408,512]{2,1,0:T(8,128)S(1)} %copy-done.4, f32[1408,512]{1,0:T(8,128)S(1)} %copy-done.10), kind=kLoop, calls=%fused_computation.11 | loop fusion | flops 4324864 | bytes 8658432 | tf_op jit(solution)/shard_map/reduce_sum | solution.py:53
  88.0 20.4 %all-reduce.2 = (f32[]{:T(128)}, f32[1408]{0:T(1024)S(1)}, f32[1408]{0:T(1024)S(1)}, f32[]{:T(128)}, f32[1408]{0:T(1024)S(1)}, /*index=5*/f32[1408]{0:T(1024)S(1...) all-reduce(f32[]{:T(128)} %get-tuple-element.70, ...), channel_id=1, replica_groups=mesh['fs'=4,'tp'=4,'rep'=2] {'fs'}, use_global_device_ids=true, to_apply=%region_6.0 | all-reduce | flops 7684 | bytes 61472 | tf_op jit(solution)/shard_map/psum | solution.py:54
  111.0 0.6 divide_reduce_fusion.1
  112.2 0.6 divide_reduce_fusion.3
  113.5 0.6 divide_reduce_fusion.2
  114.8 0.6 divide_reduce_fusion
  116.1 8.0 %all-reduce = (f32[]{:T(128)}, f32[]{:T(128)}, f32[]{:T(128)}, f32[]{:T(128)}) all-reduce(f32[]{:T(128)S(6)} %mul.202, f32[]{:T(128)S(6)} %mul.215, f32[]{:T(128)S(6)} %mul.229, f32[]{:T(128)S(6)} %mul.243), channel_id=1, replica_groups=mesh['fs'=4,'tp'=4,'rep'=2] {'tp'}, use_global_device_ids=true, to_apply=%region_10.0 | all-reduce | flops 4 | bytes 32 | tf_op jit(solution)/shard_map/psum | solution.py:65
  126.8 0.0 copy-start.1
  126.9 3.0 %divide_subtract_fusion.3 = f32[512,512]{1,0:T(8,128)} fusion(f32[512,512]{1,0:T(8,128)} %param.35, f32[512,512]{1,0:T(8,128)} %get-tuple-element.57, f32[]{:T(128)S(6)} %max.15, f32[]{:T(128)S(6)} %div.188, f32[512]{0:T(512)S(1)} %get-tuple-element.49, f32[512]{0:T(512)S(1)} %get-tuple-element.59), kind=kLoop, calls=%fused_computation.19 | loop fusion | flops 1572864 | bytes 3149832 | tf_op jit(solution)/shard_map/sub | solution.py:70
  129.8 4.3 %divide_subtract_fusion.2 = f32[512,1408]{1,0:T(8,128)} fusion(f32[512,1408]{1,0:T(8,128)} %param.20, f32[512,1408]{1,0:T(8,128)S(1)} %copy-done.1, f32[]{:T(128)S(6)} %max.12, f32[]{:T(128)S(6)} %div.154, f32[1408]{0:T(1024)S(1)} %get-tuple-element.55, f32[512]{0:T(512)S(1)} %get-tuple-element.71), kind=kLoop, calls=%fused_computation.7 | loop fusion | flops 4325376 | bytes 8658440 | tf_op jit(solution)/shard_map/sub | solution.py:70
  134.2 0.0 copy-start.2
  134.2 2.3 %divide_subtract_fusion.1 = f32[512,1408]{1,0:T(8,128)} fusion(f32[512,1408]{1,0:T(8,128)S(1)} %copy-done.11, f32[512,1408]{1,0:T(8,128)S(1)} %get-tuple-element.65, f32[]{:T(128)S(6)} %max.13, f32[]{:T(128)S(6)} %div.165, f32[1408]{0:T(1024)S(1)} %get-tuple-element.53, f32[512]{0:T(512)S(1)} %get-tuple-element.73), kind=kLoop, calls=%fused_computation.5 | loop fusion | flops 4325376 | bytes 8658440 | tf_op jit(solution)/shard_map/sub | solution.py:70
  136.5 1.4 copy-done.12
  137.9 2.3 %divide_subtract_fusion = f32[1408,512]{1,0:T(8,128)} fusion(f32[1408,512]{1,0:T(8,128)S(1)} %copy-done.12, f32[1408,512]{1,0:T(8,128)S(1)} %copy-done.2, f32[]{:T(128)S(6)} %max.14, f32[]{:T(128)S(6)} %div.176, f32[512]{0:T(512)S(1)} %get-tuple-element.51, f32[1408]{0:T(1024)S(1)} %get-tuple-element.63), kind=kLoop, calls=%fused_computation.3 | loop fusion | flops 4325376 | bytes 8658440 | tf_op jit(solution)/shard_map/sub | solution.py:70
  (53 shorter events, 0.1 us)
Async XLA Ops:
  7.2 47.6 %all-reduce.6.cloned.1.call-start = ((), (), s32[]{:S(2)}) async-start(), calls=%async_computation | async-start | bytes 19398656 | tf_op jit(solution)/shard_map/psum | solution.py:39
  54.8 3.9 %copy-start.6 = (f32[1,512,1408]{2,1,0:T(8,128)S(1)}, f32[1,512,1408]{2,1,0:T(8,128)}, u32[]{:S(2)}) copy-start(f32[1,512,1408]{2,1,0:T(8,128)} %get-tuple-element.45) | copy-start | bytes 8650756
  56.4 2.8 %copy-start.3 = (f32[1,1408,512]{2,1,0:T(8,128)S(1)}, f32[1,1408,512]{2,1,0:T(8,128)}, u32[]{:S(2)}) copy-start(f32[1,1408,512]{2,1,0:T(8,128)} %get-tuple-element.46) | copy-start | bytes 8650756
  58.7 17.3 %copy-start.27 = (f32[512]{0:T(512)S(1)}, f32[512]{0:T(512)}, u32[]{:S(2)}) copy-start(f32[512]{0:T(512)} %param.23) | copy-start | bytes 6148
  58.7 17.9 %copy-start.28 = (f32[512]{0:T(512)S(1)}, f32[512]{0:T(512)}, u32[]{:S(2)}) copy-start(f32[512]{0:T(512)} %param.38) | copy-start | bytes 6148
  58.8 17.9 %copy-start.29 = (f32[512]{0:T(512)S(1)}, f32[512]{0:T(512)}, u32[]{:S(2)}) copy-start(f32[512]{0:T(512)} %param.28) | copy-start | bytes 6148
  59.1 18.1 %copy-start.7 = (f32[1,512,512]{2,1,0:T(8,128)S(1)}, f32[1,512,512]{2,1,0:T(8,128)}, u32[]{:S(2)}) copy-start(f32[1,512,512]{2,1,0:T(8,128)} %get-tuple-element.47) | copy-start | bytes 3145732
  59.2 18.1 %copy-start.13 = (f32[512,512]{1,0:T(8,128)S(1)}, f32[512,512]{1,0:T(8,128)}, u32[]{:S(2)}) copy-start(f32[512,512]{1,0:T(8,128)} %param.36) | copy-start | bytes 3145732
  76.0 2.4 %copy-start.8 = (f32[512,1408]{1,0:T(8,128)S(1)}, f32[512,1408]{1,0:T(8,128)}, u32[]{:S(2)}) copy-start(f32[512,1408]{1,0:T(8,128)} %param.26) | copy-start | bytes 8650756
  76.6 53.2 %copy-start.18 = (f32[512]{0:T(512)}, f32[512]{0:T(512)S(1)}, u32[]{:S(2)}) copy-start(f32[512]{0:T(512)S(1)} %get-tuple-element.71) | copy-start | bytes 6148
  77.2 49.6 %copy-start.17 = (f32[512]{0:T(512)}, f32[512]{0:T(512)S(1)}, u32[]{:S(2)}) copy-start(f32[512]{0:T(512)S(1)} %get-tuple-element.59) | copy-start | bytes 6148
  77.2 56.9 %copy-start.19 = (f32[512]{0:T(512)}, f32[512]{0:T(512)S(1)}, u32[]{:S(2)}) copy-start(f32[512]{0:T(512)S(1)} %get-tuple-element.73) | copy-start | bytes 6148
  78.5 2.7 %copy-start.5 = (f32[1,512,1408]{2,1,0:T(8,128)S(1)}, f32[1,512,1408]{2,1,0:T(8,128)}, u32[]{:S(2)}) copy-start(f32[1,512,1408]{2,1,0:T(8,128)} %get-tuple-element.44) | copy-start | bytes 8650756
  78.5 3.6 %copy-start.9 = (f32[512,1408]{1,0:T(8,128)S(1)}, f32[512,1408]{1,0:T(8,128)}, u32[]{:S(2)}) copy-start(f32[512,1408]{1,0:T(8,128)} %param.21) | copy-start | bytes 8650756
  81.1 53.1 %copy-start = (f32[512,1408]{1,0:T(8,128)}, f32[512,1408]{1,0:T(8,128)S(1)}, u32[]{:S(2)}) copy-start(f32[512,1408]{1,0:T(8,128)S(1)} %get-tuple-element.65) | copy-start | bytes 8650756
  82.0 2.2 %copy-start.21 = (f32[1408]{0:T(1024)S(1)}, f32[1408]{0:T(1024)}, u32[]{:S(2)}) copy-start(f32[1408]{0:T(1024)} %param.33) | copy-start | bytes 16900
  82.0 2.8 %copy-start.4 = (f32[1,1408,512]{2,1,0:T(8,128)S(1)}, f32[1,1408,512]{2,1,0:T(8,128)}, u32[]{:S(2)}) copy-start(f32[1,1408,512]{2,1,0:T(8,128)} %get-tuple-element.46) | copy-start | bytes 8650756
  82.0 3.8 %copy-start.10 = (f32[1408,512]{1,0:T(8,128)S(1)}, f32[1408,512]{1,0:T(8,128)}, u32[]{:S(2)}) copy-start(f32[1408,512]{1,0:T(8,128)} %param.31) | copy-start | bytes 8650756
  84.8 51.7 %copy-start.14 = (f32[1408]{0:T(1024)}, f32[1408]{0:T(1024)S(1)}, u32[]{:S(2)}) copy-start(f32[1408]{0:T(1024)S(1)} %get-tuple-element.63) | copy-start | bytes 16900
  85.8 25.2 %copy-start.22 = (f32[1408]{0:T(1024)S(1)}, f32[1408]{0:T(1024)}, u32[]{:S(2)}) copy-start(f32[1408]{0:T(1024)} %param.24) | copy-start | bytes 16900
  85.8 26.5 %copy-start.25 = (f32[512]{0:T(512)S(1)}, f32[512]{0:T(512)}, u32[]{:S(2)}) copy-start(f32[512]{0:T(512)} %param.34) | copy-start | bytes 6148
  85.8 27.7 %copy-start.26 = (f32[512]{0:T(512)S(1)}, f32[512]{0:T(512)}, u32[]{:S(2)}) copy-start(f32[512]{0:T(512)} %param.39) | copy-start | bytes 6148
  85.8 29.0 %copy-start.23 = (f32[1408]{0:T(1024)S(1)}, f32[1408]{0:T(1024)}, u32[]{:S(2)}) copy-start(f32[1408]{0:T(1024)} %param.29) | copy-start | bytes 16900
  111.6 22.5 %copy-start.15 = (f32[1408]{0:T(1024)}, f32[1408]{0:T(1024)S(1)}, u32[]{:S(2)}) copy-start(f32[1408]{0:T(1024)S(1)} %get-tuple-element.55) | copy-start | bytes 16900
  112.9 23.6 %copy-start.20 = (f32[512]{0:T(512)}, f32[512]{0:T(512)S(1)}, u32[]{:S(2)}) copy-start(f32[512]{0:T(512)S(1)} %get-tuple-element.51) | copy-start | bytes 6148
  114.1 20.0 %copy-start.24 = (f32[512]{0:T(512)}, f32[512]{0:T(512)S(1)}, u32[]{:S(2)}) copy-start(f32[512]{0:T(512)S(1)} %get-tuple-element.49) | copy-start | bytes 6148
  115.4 18.7 %copy-start.16 = (f32[1408]{0:T(1024)}, f32[1408]{0:T(1024)S(1)}, u32[]{:S(2)}) copy-start(f32[1408]{0:T(1024)S(1)} %get-tuple-element.53) | copy-start | bytes 16900
  126.8 3.0 %copy-start.1 = (f32[512,1408]{1,0:T(8,128)S(1)}, f32[512,1408]{1,0:T(8,128)}, u32[]{:S(2)}) copy-start(f32[512,1408]{1,0:T(8,128)} %get-tuple-element.69) | copy-start | bytes 8650756
  129.8 4.3 %copy-start.11 = (f32[512,1408]{1,0:T(8,128)S(1)}, f32[512,1408]{1,0:T(8,128)}, u32[]{:S(2)}) copy-start(f32[512,1408]{1,0:T(8,128)} %param.25) | copy-start | bytes 8650756
  134.2 2.3 %copy-start.2 = (f32[1408,512]{1,0:T(8,128)S(1)}, f32[1408,512]{1,0:T(8,128)}, u32[]{:S(2)}) copy-start(f32[1408,512]{1,0:T(8,128)} %get-tuple-element.61) | copy-start | bytes 8650756
  134.2 3.7 %copy-start.12 = (f32[1408,512]{1,0:T(8,128)S(1)}, f32[1408,512]{1,0:T(8,128)}, u32[]{:S(2)}) copy-start(f32[1408,512]{1,0:T(8,128)} %param.30) | copy-start | bytes 8650756
Sparse Core Ops, SparseCore 0:
  10.8 43.9 all-reduce.5
where the time goes:
time: 147 us
  waiting for transfers between devices  47.6 us (32%)
  blocking collectives  44.9 us (31%)
  other arithmetic  28.9 us (20%)
  between operations  22.2 us (15%)
  local copies, waits for them, and re-layouts  3.44 us (2%)
    psum x1, waiting for transfers between devices, body(): lax.psum((partials[0], partials[1], partials[2], partials[3]), 'rep')  46.9 us
    psum x1, blocking collectives, body(): outcome = lax.psum(column_local + row_mass + shares, 'fs')  20.4 us
    psum x1, blocking collectives, body(): row_total = lax.psum(row_local, 'tp')  16.5 us
    sub x4, other arithmetic, body(): weights_next.append(weights[k] - step_rate * updates[k] / factor)  11.9 us
    reduce_sum x4, other arithmetic, body(): jnp.sum(m * m / r[:, None], axis=0)  8.17 us
    psum x1, blocking collectives, body(): totals = lax.psum(pieces, 'tp')  7.99 us
    reduce_sum x4, other arithmetic, body(): column_local = tuple((jnp.sum(item, axis=0) for item in squares))  4.65 us
    unnamed x60, local copies, waits for them, and re-layouts  3.44 us
  transfers between devices with their start and end apart: 1, of which 1 were waited for; matrix products, arithmetic and copies ran while one was open for 0% of the time, Pallas kernels for 0%

commit v1 on v0

v1 whole, which is shorter than its diff:
```python
import functools
import math

import jax
import jax.numpy as jnp
from jax import lax
from jax.experimental import pallas as pl
from jax.experimental.pallas import tpu as pltpu
from jax.sharding import PartitionSpec as P

momentum_decay = 0.9
moment_decay = 0.95
clip_level = 0.25
step_rate = 0.1
MESH = pl.DeviceIdType.MESH
LANES = 128


def chunk_rows(height):
    return LANES if height % LANES == 0 else height


def fold(x):
    return jnp.sum(x.reshape(x.shape[0] // 8, 8, x.shape[1]), axis=0)


def to_lanes(x):
    rows = x.shape[0]
    if rows < LANES:
        x = jnp.concatenate([x, jnp.zeros((LANES - rows, LANES), x.dtype)], axis=0)
    return jnp.sum(x.T, axis=0, keepdims=True)


def to_rows(x, rows):
    return jnp.broadcast_to(x, (LANES, LANES)).T[:rows]


def gather_kernel(sizes, n_fs, n_tp, *refs):
    n_all = n_fs * n_tp
    ins, refs = refs[:20], refs[20:]
    outs, refs = refs[:20], refs[20:]
    own, refs = refs[:4], refs[4:]
    other, refs = refs[:4], refs[4:]
    row_all, refs = refs[:4], refs[4:]
    column_part, refs = refs[:4], refs[4:]
    column_all, refs = refs[:4], refs[4:]
    share_all, refs = refs[:4], refs[4:]
    (own_sem, other_send, other_recv, momentum_sem, weight_sem,
     row_send, row_recv, column_send, column_recv, share_send, share_recv) = refs
    fs, tp, rep = lax.axis_index("fs"), lax.axis_index("tp"), lax.axis_index("rep")
    me = fs * n_tp + tp
    barrier = pltpu.get_barrier_semaphore()

    def place(d):
        lin = lax.rem(me + d, n_all)
        return {"fs": lax.div(lin, n_tp), "tp": lax.rem(lin, n_tp)}

    pl.semaphore_signal(barrier, inc=1, device_id={"rep": 1 - rep}, device_id_type=MESH)

    @pl.loop(1, n_all)
    def _(d):
        pl.semaphore_signal(barrier, inc=1, device_id=place(d), device_id_type=MESH)

    base = [0]
    for height, width in sizes:
        base.append(base[-1] + height // chunk_rows(height))

    def span(k, c):
        rows = chunk_rows(sizes[k][0])
        return pl.ds(pl.multiple_of(c * rows, rows), rows)

    def load(k, c):
        return pltpu.make_async_copy(
            ins[5 * k + 2].at[0, span(k, c)], own[k].at[span(k, c)], own_sem.at[base[k] + c])

    def send(k, c):
        return pltpu.make_async_remote_copy(
            src_ref=ins[5 * k + 2].at[0, span(k, c)], dst_ref=other[k].at[span(k, c)],
            send_sem=other_send.at[base[k] + c], recv_sem=other_recv.at[base[k] + c],
            device_id={"rep": 1 - rep}, device_id_type=MESH)

    def load_momentum(k, c):
        return pltpu.make_async_copy(
            ins[5 * k + 1].at[span(k, c)], outs[5 * k + 1].at[span(k, c)], momentum_sem.at[base[k] + c])

    def load_weight(k):
        return pltpu.make_async_copy(ins[5 * k], outs[5 * k], weight_sem.at[k])

    def each(k, f):
        @pl.loop(0, base[k + 1] - base[k])
        def _(c):
            f(k, c)

    each(0, lambda k, c: load(k, c).start())
    each(0, lambda k, c: load_momentum(k, c).start())
    pl.semaphore_wait(barrier, n_all)
    for k in range(4):
        each(k, lambda k, c: send(k, c).start())
    for k in range(1, 4):
        each(k, lambda k, c: load(k, c).start())
        each(k, lambda k, c: load_momentum(k, c).start())
    for k in range(4):
        load_weight(k).start()

    def accumulate(k):
        height, width = sizes[k]
        rows, tiles = chunk_rows(height), width // LANES
        column_part[k][...] = jnp.zeros_like(column_part[k])

        @pl.loop(0, height // rows)
        def _(c):
            load(k, c).wait()
            load_momentum(k, c).wait()
            send(k, c).wait_recv()
            part = jnp.zeros((rows, LANES), jnp.float32)
            for j in range(tiles):
                at = (span(k, c), pl.ds(j * LANES, LANES))
                grad = own[k][at] + other[k][at]
                outs[5 * k + 1][at] = momentum_decay * outs[5 * k + 1][at] + (1.0 - momentum_decay) * grad
                square = grad * grad
                part = part + square
                column_part[k][:, pl.ds(j * LANES, LANES)] += fold(square)
            row_all[k][tp, pl.ds(c, 1)] = to_lanes(part)

        column_all[k][fs] = jnp.sum(column_part[k][...], axis=0, keepdims=True)

    def row_copy(k, d):
        peer = lax.rem(tp + d, n_tp)
        return pltpu.make_async_remote_copy(
            src_ref=row_all[k].at[tp], dst_ref=row_all[k].at[tp],
            send_sem=row_send.at[k, d], recv_sem=row_recv.at[k, d],
            device_id={"tp": peer}, device_id_type=MESH)

    def column_copy(k, d):
        peer = lax.rem(fs + d, n_fs)
        return pltpu.make_async_remote_copy(
            src_ref=column_all[k].at[fs], dst_ref=column_all[k].at[fs],
            send_sem=column_send.at[k, d], recv_sem=column_recv.at[k, d],
            device_id={"fs": peer}, device_id_type=MESH)

    def share_copy(k, d):
        return pltpu.make_async_remote_copy(
            src_ref=share_all[k].at[me], dst_ref=share_all[k].at[me],
            send_sem=share_send.at[k, d], recv_sem=share_recv.at[k, d],
            device_id=place(d), device_id_type=MESH)

    def send_sums(k):
        @pl.loop(1, n_fs)
        def _(d):
            column_copy(k, d).start()

        @pl.loop(1, n_tp)
        def _(d):
            row_copy(k, d).start()

    def moments(k):
        height, width = sizes[k]
        rows, tiles = chunk_rows(height), width // LANES

        @pl.loop(1, n_tp)
        def _(d):
            row_copy(k, d).wait_recv()

        @pl.loop(1, n_fs)
        def _(d):
            column_copy(k, d).wait_recv()

        row_total = jnp.sum(row_all[k][...], axis=0) / (width * n_tp)
        row_next = moment_decay * ins[5 * k + 3][...] + (1.0 - moment_decay) * row_total
        outs[5 * k + 2][...] = row_next
        column_total = jnp.sum(column_all[k][...], axis=0) / (height * n_fs)
        column_next = moment_decay * ins[5 * k + 4][...] + (1.0 - moment_decay) * column_total
        outs[5 * k + 3][...] = column_next
        lane = lax.broadcasted_iota(jnp.int32, row_next.shape, 1)
        mass = jnp.sum(jnp.where(lane < rows, row_next, 0.0), axis=0, keepdims=True)

        def step(c, sums):
            inverse = to_rows(1.0 / outs[5 * k + 2][pl.ds(c, 1)], rows)
            new = []
            for j in range(tiles):
                m = outs[5 * k + 1][span(k, c), pl.ds(j * LANES, LANES)]
                new.append(sums[j] + fold(m * m * inverse))
            return tuple(new)

        zero = jnp.zeros((8, LANES), jnp.float32)
        sums = lax.fori_loop(0, height // rows, step, (zero,) * tiles)
        share = zero
        for j in range(tiles):
            share = share + sums[j] / outs[5 * k + 3][:, pl.ds(j * LANES, LANES)]
        share = jnp.sum(share, axis=0, keepdims=True)
        share_all[k][me] = jnp.concatenate([share, mass], axis=0)

    def send_share(k):
        @pl.loop(1, n_all)
        def _(d):
            share_copy(k, d).start()

    def scale(k):
        height, width = sizes[k]

        @pl.loop(1, n_all)
        def _(d):
            share_copy(k, d).wait_recv()

        total = jnp.sum(share_all[k][...], axis=0)
        total = jnp.sum(total, axis=1, keepdims=True)
        row_mean = total[1:2] / (height * n_fs * n_tp)
        spread = jnp.sqrt(row_mean * total[0:1] / (height * n_fs * width * n_tp))
        factor = jnp.maximum(1.0, spread / clip_level)
        outs[5 * k + 4][...] = jnp.broadcast_to(step_rate * jnp.sqrt(row_mean) / factor, (1, LANES))

    for k in range(4):
        accumulate(k)
        send_sums(k)
        if k >= 1:
            moments(k - 1)
            send_share(k - 1)
        if k >= 2:
            scale(k - 2)
    moments(3)
    send_share(3)
    scale(2)
    scale(3)
    for k in range(4):
        load_weight(k).wait()
        each(k, lambda k, c: send(k, c).wait_send())

        @pl.loop(1, n_tp)
        def _(d):
            row_copy(k, d).wait_send()

        @pl.loop(1, n_fs)
        def _(d):
            column_copy(k, d).wait_send()

        @pl.loop(1, n_all)
        def _(d):
            share_copy(k, d).wait_send()


def write_kernel(sizes, *refs):
    ins, refs = refs[:20], refs[20:]
    outs, refs = refs[:16], refs[16:]
    weight_next, refs = refs[:4], refs[4:]
    momentum_sem, weight_sem = refs

    def put_momentum(k):
        return pltpu.make_async_copy(ins[5 * k + 1], outs[4 * k + 1], momentum_sem.at[k])

    base = [0]
    for height, width in sizes:
        base.append(base[-1] + height // chunk_rows(height))

    def span(k, c):
        rows = chunk_rows(sizes[k][0])
        return pl.ds(pl.multiple_of(c * rows, rows), rows)

    def put_weight(k, c):
        return pltpu.make_async_copy(
            weight_next[k].at[span(k, c)], outs[4 * k].at[span(k, c)], weight_sem.at[base[k] + c])

    for k in range(4):
        put_momentum(k).start()
    for k, (height, width) in enumerate(sizes):
        rows = chunk_rows(height)
        outs[4 * k + 2][...] = ins[5 * k + 2][:, :rows]
        outs[4 * k + 3][...] = ins[5 * k + 3][...]

        @pl.loop(0, height // rows)
        def _(c):
            row_factor = to_rows(lax.rsqrt(ins[5 * k + 2][pl.ds(c, 1)]), rows)
            for j in range(width // LANES):
                at = (span(k, c), pl.ds(j * LANES, LANES))
                column_factor = lax.rsqrt(ins[5 * k + 3][:, pl.ds(j * LANES, LANES)]) * ins[5 * k + 4][...]
                weight_next[k][at] = ins[5 * k][at] - ins[5 * k + 1][at] * row_factor * column_factor
            put_weight(k, c).start()

    for k, (height, width) in enumerate(sizes):
        put_momentum(k).wait()

        @pl.loop(0, height // chunk_rows(height))
        def _(c):
            put_weight(k, c).wait()


def body(n_fs, n_tp, *arrays):
    f32 = jnp.float32
    sizes = tuple(arrays[5 * k].shape for k in range(4))
    chunks = [height // chunk_rows(height) for height, _ in sizes]
    n_all, total = n_fs * n_tp, sum(chunks)
    operands, middle = [], []
    in_specs = []
    hbm, vmem = pl.BlockSpec(memory_space=pl.ANY), pl.BlockSpec(memory_space=pltpu.VMEM)
    for k, (height, width) in enumerate(sizes):
        w, m, g, r, c = arrays[5 * k:5 * k + 5]
        rows = chunk_rows(height)
        r = r.reshape(chunks[k], rows)
        if rows < LANES:
            r = jnp.pad(r, ((0, 0), (0, LANES - rows)), constant_values=1.0)
        operands += [w, m, g, r, c.reshape(1, width)]
        in_specs += [hbm, hbm, hbm, vmem, vmem]
        middle += [pltpu.VMEM((height, width), f32), pltpu.VMEM((height, width), f32),
                   pltpu.VMEM((chunks[k], LANES), f32), pltpu.VMEM((1, width), f32), pltpu.VMEM((1, LANES), f32)]
    scratch = [pltpu.VMEM(s, f32) for s in sizes] + [pltpu.VMEM(s, f32) for s in sizes]
    scratch += [pltpu.VMEM((n_tp, n, LANES), f32) for n in chunks]
    scratch += [pltpu.VMEM((8, s[1]), f32) for s in sizes]
    scratch += [pltpu.VMEM((n_fs, 1, s[1]), f32) for s in sizes]
    scratch += [pltpu.VMEM((n_all, 2, LANES), f32) for s in sizes]
    dma = pltpu.SemaphoreType.DMA
    scratch += [dma((total,)), dma((total,)), dma((total,)), dma((total,)), dma((4,))]
    scratch += [dma((4, n_tp)), dma((4, n_tp)), dma((4, n_fs)), dma((4, n_fs)), dma((4, n_all)), dma((4, n_all))]
    block = 4 * sum(h * w for h, w in sizes)
    slack = 4 << 20
    middle = pl.pallas_call(
        functools.partial(gather_kernel, sizes, n_fs, n_tp),
        out_shape=middle,
        in_specs=in_specs,
        out_specs=[vmem] * 20,
        scratch_shapes=scratch,
        compiler_params=pltpu.CompilerParams(
            collective_id=0, has_side_effects=True, vmem_limit_bytes=2 * block + slack),
        name="gather",
    )(*operands)
    out_shape, out_specs = [], []
    for k, (height, width) in enumerate(sizes):
        rows = chunk_rows(height)
        out_shape += [jax.ShapeDtypeStruct((height, width), f32)] * 2
        out_shape += [jax.ShapeDtypeStruct((chunks[k], rows), f32), jax.ShapeDtypeStruct((1, width), f32)]
        out_specs += [hbm, hbm, vmem, vmem]
    outs = pl.pallas_call(
        functools.partial(write_kernel, sizes),
        out_shape=out_shape,
        in_specs=[vmem] * 20,
        out_specs=out_specs,
        scratch_shapes=[pltpu.VMEM(s, f32) for s in sizes] + [dma((4,)), dma((total,))],
        compiler_params=pltpu.CompilerParams(vmem_limit_bytes=block + slack),
        name="write",
    )(*middle)
    results = []
    for k in range(4):
        results += [outs[4 * k], outs[4 * k + 1], outs[4 * k + 2].reshape(-1), outs[4 * k + 3].reshape(-1)]
    return tuple(results)


def solution(mesh):
    matrix, partial, row, column = P("fs", "tp"), P("rep", "fs", "tp"), P("fs"), P("tp")
    return jax.shard_map(
        functools.partial(body, mesh.shape["fs"], mesh.shape["tp"]),
        mesh=mesh,
        in_specs=(matrix, matrix, partial, row, column) * 4,
        out_specs=(matrix, matrix, row, column) * 4,
        check_vma=False,
    )
```

time: 147 us -> 58.1 us (0.40)
  waiting for transfers between devices: 47.6 us -> 0 us
  blocking collectives: 44.9 us -> 0 us
  Pallas kernels: 0 us -> 41 us
  other arithmetic: 28.9 us -> 1.24 us
  between operations: 22.2 us -> 0.68 us
  local copies, waits for them, and re-layouts: 3.44 us -> 14.6 us
    psum x1 -> x0, waiting for transfers between devices: 46.9 us -> none  [body(): lax.psum((partials[0], partials[1], partials[2], partials[3]), 'rep')]
    psum x3 -> x0, blocking collectives: 44.9 us -> none  [the longest x1 20.4 us: body(): outcome = lax.psum(column_local + row_mass + shares, 'fs')]
    pallas_call x0 -> x2, Pallas kernels: none -> 41 us  [the longest x1 33.5 us: body(): pl.pallas_call(functools.partial(gather_kernel, sizes, n_fs, n_tp), out_s...]
    reduce_sum x15 -> x0, other arithmetic: 17.1 us -> none  [the longest x4 8.17 us: body(): jnp.sum(m * m / r[:, None], axis=0)]
    sub x4 -> x0, other arithmetic: 11.9 us -> none  [body(): weights_next.append(weights[k] - step_rate * updates[k] / factor)]
    unnamed x60 -> x24, local copies, waits for them, and re-layouts: 3.44 us -> 13.2 us
  transfers between devices with their start and end apart: 1 -> 0, of which waited for: 1 -> 0; matrix products, arithmetic and copies ran while one was open for 0% -> 0% of each run, Pallas kernels for 0% -> 0%
where the time goes in v1:
time: 58.1 us; the launch traced here: 57.5 us
  Pallas kernels  41 us (71%)
  local copies, waits for them, and re-layouts  14.6 us (25%)
  other arithmetic  1.24 us (2%)
  between operations  0.68 us (1%)
    pallas_call x1, Pallas kernels, body(): pl.pallas_call(functools.partial(gather_kernel, sizes, n_fs, n_tp), out_s...  33.5 us
    unnamed x24, local copies, waits for them, and re-layouts  13.2 us
    pallas_call x1, Pallas kernels, body(): pl.pallas_call(functools.partial(write_kernel, sizes), out_shape=out_shap...  7.52 us
    reshape x2, local copies, waits for them, and re-layouts, body(): operands += [w, m, g, r, c.reshape(1, width)]  1.4 us
    pallas_call x2, other arithmetic, body(): pl.pallas_call(functools.partial(write_kernel, sizes), out_shape=out_shap...  1.24 us

profile of v1, /device:TPU:0, one launch (start us, length us, event | category | flops | bytes accessed | tf_op | source)
XLA Modules:
  0.0 57.5 jit_solution(18094366455251825988)
XLA Ops:
  0.6 0.7 %reshape.81.refs_4_ = f32[1,1408]{1,0:T(1,128)S(1)} reshape(f32[1408]{0:T(1024)} %param.24) | data formatting | bytes 11264 | tf_op jit(solution)/shard_map/reshape | solution.py:300
  1.3 0.7 %reshape.83.refs_9_ = f32[1,1408]{1,0:T(1,128)S(1)} reshape(f32[1408]{0:T(1024)} %param.29) | data formatting | bytes 11264 | tf_op jit(solution)/shard_map/reshape | solution.py:300
  2.0 0.0 copy-start
  2.1 1.8 %copy-done = f32[512,1408]{1,0:T(8,128)S(1)} copy-done((f32[512,1408]{1,0:T(8,128)S(1)}, f32[512,1408]{1,0:T(8,128)}, u32[]{:S(2)}) %copy-start) | copy-done | bytes 2883608
  3.9 0.0 copy-start.1
  3.9 1.8 %copy-done.1 = f32[512,1408]{1,0:T(8,128)S(1)} copy-done((f32[512,1408]{1,0:T(8,128)S(1)}, f32[512,1408]{1,0:T(8,128)}, u32[]{:S(2)}) %copy-start.1) | copy-done | bytes 2883608
  5.7 0.0 copy-start.2
  5.7 1.8 %copy-done.2 = f32[1,512,1408]{2,1,0:T(8,128)S(1)} copy-done((f32[1,512,1408]{2,1,0:T(8,128)S(1)}, f32[1,512,1408]{2,1,0:T(8,128)}, u32[]{:S(2)}) %copy-start.2) | copy-done | bytes 2883608
  7.5 0.0 copy-start.3
  7.5 1.2 %copy-done.3 = f32[512,512]{1,0:T(8,128)S(1)} copy-done((f32[512,512]{1,0:T(8,128)S(1)}, f32[512,512]{1,0:T(8,128)}, u32[]{:S(2)}) %copy-start.3) | copy-done | bytes 1048600
  8.7 0.0 copy-start.4
  8.7 1.2 %copy-done.4 = f32[512,512]{1,0:T(8,128)S(1)} copy-done((f32[512,512]{1,0:T(8,128)S(1)}, f32[512,512]{1,0:T(8,128)}, u32[]{:S(2)}) %copy-start.4) | copy-done | bytes 1048600
  9.9 0.0 copy-start.5
  9.9 1.2 %copy-done.5 = f32[1,512,512]{2,1,0:T(8,128)S(1)} copy-done((f32[1,512,512]{2,1,0:T(8,128)S(1)}, f32[1,512,512]{2,1,0:T(8,128)}, u32[]{:S(2)}) %copy-start.5) | copy-done | bytes 1048600
  11.2 0.0 copy-start.6
  11.2 0.7 %copy-done.6 = f32[1408]{0:T(1024)S(1)} copy-done((f32[1408]{0:T(1024)S(1)}, f32[1408]{0:T(1024)}, u32[]{:S(2)}) %copy-start.6) | copy-done | bytes 5656
  11.9 0.0 copy-start.7
  11.9 0.7 %copy-done.7 = f32[512]{0:T(512)S(1)} copy-done((f32[512]{0:T(512)S(1)}, f32[512]{0:T(512)}, u32[]{:S(2)}) %copy-start.7) | copy-done | bytes 2072
  12.5 0.0 copy-start.8
  12.6 0.7 %copy-done.8 = f32[512]{0:T(512)S(1)} copy-done((f32[512]{0:T(512)S(1)}, f32[512]{0:T(512)}, u32[]{:S(2)}) %copy-start.8) | copy-done | bytes 2072
  13.2 0.0 copy-start.9
  13.2 0.7 %copy-done.9 = f32[512]{0:T(512)S(1)} copy-done((f32[512]{0:T(512)S(1)}, f32[512]{0:T(512)}, u32[]{:S(2)}) %copy-start.9) | copy-done | bytes 2072
  13.9 0.0 copy-start.10
  13.9 0.7 %copy-done.10 = f32[512]{0:T(512)S(1)} copy-done((f32[512]{0:T(512)S(1)}, f32[512]{0:T(512)}, u32[]{:S(2)}) %copy-start.10) | copy-done | bytes 2072
  14.6 0.0 copy-start.11
  14.6 0.7 %copy-done.11 = f32[512]{0:T(512)S(1)} copy-done((f32[512]{0:T(512)S(1)}, f32[512]{0:T(512)}, u32[]{:S(2)}) %copy-start.11) | copy-done | bytes 2072
  15.3 33.5 %gather.1 = (f32[512,1408]{1,0:T(8,128)S(1)}, f32[512,1408]{1,0:T(8,128)S(1)}, f32[4,128]{1,0:T(4,128)S(1)}, f32[1,1408]{1,0:T(1,128)S(1)}, f32[1,128]{1,0:T(1,1...) custom-call(f32[512,1408]{1,0:T(8,128)S(1)} %copy-done, ...), custom_call_target="tpu_custom_call" | custom-call | tf_op jit(solution)/shard_map/gather/pallas_call | solution.py:314
  48.8 7.5 %write.1 = (f32[512,1408]{1,0:T(8,128)}, f32[512,1408]{1,0:T(8,128)}, f32[4,128]{1,0:T(4,128)}, f32[1,1408]{1,0:T(1,128)S(1)}, f32[512,1408]{1,0:T(8,128)}, /*in...) custom-call(f32[512,1408]{1,0:T(8,128)S(1)} %get-tuple-element.52.re, ...), custom_call_target="tpu_custom_call" | custom-call | tf_op jit(solution)/shard_map/write/pallas_call | solution.py:330
  56.3 0.6 %reduce = f32[1408]{0:T(1024)} reduce(f32[1,1408]{1,0:T(1,128)S(1)} %get-tuple-element.75, f32[]{:T(128)} %constant.4), dimensions={0}, to_apply=%get-tuple-element.75.reduce_sub_computation | reduce | bytes 11268 | tf_op jit(solution)/shard_map/write/pallas_call | solution.py:330
  56.9 0.6 %reduce.1 = f32[1408]{0:T(1024)} reduce(f32[1,1408]{1,0:T(1,128)S(1)} %get-tuple-element.79, f32[]{:T(128)} %constant.4), dimensions={0}, to_apply=%get-tuple-element.79.reduce_sub_computation | reduce | bytes 11268 | tf_op jit(solution)/shard_map/write/pallas_call | solution.py:330
Async XLA Ops:
  2.0 1.8 %copy-start = (f32[512,1408]{1,0:T(8,128)S(1)}, f32[512,1408]{1,0:T(8,128)}, u32[]{:S(2)}) copy-start(f32[512,1408]{1,0:T(8,128)} %refs_0_.1) | copy-start | bytes 8650756
  3.9 1.8 %copy-start.1 = (f32[512,1408]{1,0:T(8,128)S(1)}, f32[512,1408]{1,0:T(8,128)}, u32[]{:S(2)}) copy-start(f32[512,1408]{1,0:T(8,128)} %refs_1_.1) | copy-start | bytes 8650756
  5.7 1.8 %copy-start.2 = (f32[1,512,1408]{2,1,0:T(8,128)S(1)}, f32[1,512,1408]{2,1,0:T(8,128)}, u32[]{:S(2)}) copy-start(f32[1,512,1408]{2,1,0:T(8,128)} %refs_2_.1) | copy-start | bytes 8650756
  7.5 1.2 %copy-start.3 = (f32[512,512]{1,0:T(8,128)S(1)}, f32[512,512]{1,0:T(8,128)}, u32[]{:S(2)}) copy-start(f32[512,512]{1,0:T(8,128)} %refs_15_.1) | copy-start | bytes 3145732
  8.7 1.2 %copy-start.4 = (f32[512,512]{1,0:T(8,128)S(1)}, f32[512,512]{1,0:T(8,128)}, u32[]{:S(2)}) copy-start(f32[512,512]{1,0:T(8,128)} %refs_16_.1) | copy-start | bytes 3145732
  9.9 1.2 %copy-start.5 = (f32[1,512,512]{2,1,0:T(8,128)S(1)}, f32[1,512,512]{2,1,0:T(8,128)}, u32[]{:S(2)}) copy-start(f32[1,512,512]{2,1,0:T(8,128)} %refs_17_.1) | copy-start | bytes 3145732
  11.2 0.7 %copy-start.6 = (f32[1408]{0:T(1024)S(1)}, f32[1408]{0:T(1024)}, u32[]{:S(2)}) copy-start(f32[1408]{0:T(1024)} %param.33) | copy-start | bytes 16900
  11.9 0.7 %copy-start.7 = (f32[512]{0:T(512)S(1)}, f32[512]{0:T(512)}, u32[]{:S(2)}) copy-start(f32[512]{0:T(512)} %param.23) | copy-start | bytes 6148
  12.5 0.7 %copy-start.8 = (f32[512]{0:T(512)S(1)}, f32[512]{0:T(512)}, u32[]{:S(2)}) copy-start(f32[512]{0:T(512)} %param.28) | copy-start | bytes 6148
  13.2 0.7 %copy-start.9 = (f32[512]{0:T(512)S(1)}, f32[512]{0:T(512)}, u32[]{:S(2)}) copy-start(f32[512]{0:T(512)} %param.34) | copy-start | bytes 6148
  13.9 0.7 %copy-start.10 = (f32[512]{0:T(512)S(1)}, f32[512]{0:T(512)}, u32[]{:S(2)}) copy-start(f32[512]{0:T(512)} %param.38) | copy-start | bytes 6148
  14.6 0.7 %copy-start.11 = (f32[512]{0:T(512)S(1)}, f32[512]{0:T(512)}, u32[]{:S(2)}) copy-start(f32[512]{0:T(512)} %param.39) | copy-start | bytes 6148
